TPU v7x, 32 devices: a whole 2x2x4 slice. The times are simulated.
32 devices in a mesh: row: 8 (over z, core), col: 4 (over y, x).
Axes of the slice: x: 2, y: 2, z: 4, core: 2. Of those that a mesh axis runs over, the one named last changes fastest.
Arguments:
- tokens: bfloat16 [4096, 2048], P('row'), may hold values from -6 to 6
- out_weight: bfloat16 [2048, 2048], P(None, 'col'), may hold values from -0.125 to 0.125
Outputs:
- mixed: bfloat16 [4096, 2048], P('row', 'col')
All inputs are finite; a program needn't handle non-finite values.
Results may differ from a plain program's by a relative error of at most 0.001.
Values may be sent and summed in bfloat16 or wider, within the bound.
A program may use at most 64 MiB of HBM per device.

v0:
```python
import math

import functools

import jax
import jax.numpy as jnp
import numpy as np
from jax import lax
from jax.experimental import pallas as pl
from jax.experimental.pallas import tpu as pltpu
from jax.sharding import PartitionSpec as P

GROUPS = 4
GROUP_DIM = 512


def angles(product, period):
    return (product % period).astype(jnp.float32) * (2.0 * math.pi / period)


def plain_dot(matrix, values):
    return jnp.dot(
        matrix, values, precision=lax.Precision.HIGHEST, preferred_element_type=jnp.float32
    )


def whole_transform(whole_rows, row_count, seg_rows, length):
    few_chans = whole_rows.shape[2]
    lattice = jnp.arange(row_count, dtype=jnp.int32)
    phases = angles(lattice[:, None] * lattice[None, :], row_count)
    cosine_table = jnp.cos(phases)
    sine_table = jnp.sin(phases)
    real_in = whole_rows[0].reshape(row_count, seg_rows * few_chans)
    imag_in = whole_rows[1].reshape(row_count, seg_rows * few_chans)
    first_re = (plain_dot(cosine_table, real_in) + plain_dot(sine_table, imag_in)).reshape(
        row_count, seg_rows, few_chans
    )
    first_im = (plain_dot(cosine_table, imag_in) - plain_dot(sine_table, real_in)).reshape(
        row_count, seg_rows, few_chans
    )
    inner = jnp.arange(seg_rows, dtype=jnp.int32)
    twist = angles(lattice[:, None] * inner[None, :], length)[:, :, None]
    twist_cos = jnp.cos(twist)
    twist_sin = jnp.sin(twist)
    turned_re = twist_cos * first_re + twist_sin * first_im
    turned_im = twist_cos * first_im - twist_sin * first_re
    folded_re = jnp.transpose(turned_re, (1, 0, 2)).reshape(seg_rows, row_count * few_chans)
    folded_im = jnp.transpose(turned_im, (1, 0, 2)).reshape(seg_rows, row_count * few_chans)
    seg_phases = angles(inner[:, None] * inner[None, :], seg_rows)
    real_part = plain_dot(jnp.cos(seg_phases), folded_re) + plain_dot(
        jnp.sin(seg_phases), folded_im
    )
    return real_part.reshape(length, few_chans)


def general_body(tokens, out_weight):
    seg_rows = tokens.shape[0]
    col_width = out_weight.shape[1]
    row_count = lax.axis_size("row")
    length = seg_rows * row_count
    scaling = 1.0 / math.sqrt(length * GROUP_DIM)
    weight_wide = out_weight.astype(jnp.float32)
    lattice = jnp.arange(GROUP_DIM, dtype=jnp.int32)
    phases = angles(lattice[:, None] * lattice[None, :], GROUP_DIM)
    cosine_table = jnp.cos(phases) * scaling
    sine_table = jnp.sin(phases) * scaling
    folded_rows = []
    for group in range(GROUPS):
        group_rows = weight_wide[group * GROUP_DIM : (group + 1) * GROUP_DIM]
        folded_rows.append(
            jnp.concatenate(
                [plain_dot(cosine_table, group_rows), -plain_dot(sine_table, group_rows)], axis=1
            )
        )
    folded_map = jnp.concatenate(folded_rows, axis=0)
    spectrum = plain_dot(tokens.astype(jnp.float32), folded_map)
    stacked = jnp.stack([spectrum[:, :col_width], spectrum[:, col_width:]])
    whole_rows = lax.all_to_all(stacked, "row", split_axis=2, concat_axis=1, tiled=True)
    ordered = whole_transform(whole_rows, row_count, seg_rows, length)
    spectral = lax.all_to_all(
        ordered.astype(jnp.bfloat16), "row", split_axis=0, concat_axis=1, tiled=True
    )
    return spectral

RADIX = 8
HALF = 64
LANES = 128
EXTRA = 16
CODE = 84.0


def split_table(values):
    big = values.astype(jnp.bfloat16)
    return big, (values - big.astype(np.float64)).astype(jnp.bfloat16)


def tables(size, length):
    index = np.arange(size)
    phase = 2.0 * np.pi * ((index[:, None] * index[None, :]) % size) / size
    high, low = split_table(np.concatenate([np.cos(phase), np.sin(phase)], axis=0))
    turn = 2.0 * np.pi * (index[:, None] * np.arange(RADIX)[None, :]) / length
    twist = np.zeros((size, LANES), np.float32)
    twist[:, :RADIX] = np.cos(turn)
    twist[:, RADIX : 2 * RADIX] = np.sin(turn)
    small = np.arange(RADIX)
    eight = 2.0 * np.pi * ((small[:, None] * small[None, :]) % RADIX) / RADIX
    last = np.concatenate(
        [
            np.repeat(np.cos(eight)[:, :, None], HALF, axis=2),
            np.repeat(np.sin(eight)[:, :, None], HALF, axis=2),
        ],
        axis=2,
    ).astype(np.float32)
    inner = size // RADIX
    perm = np.zeros((size, size), np.float32)
    rows = np.arange(size)
    perm[rows, (rows % inner) * RADIX + rows // inner] = 1.0
    return high, low, twist, last, perm.astype(high.dtype)


def dot(a, b):
    return jnp.dot(a, b, preferred_element_type=jnp.float32)


def split(values):
    high = values.astype(jnp.bfloat16)
    return high, (values - high.astype(jnp.float32)).astype(jnp.bfloat16)


def peer_at(step, chip):
    upper = lax.rem(chip // 2 + 1 - step // 2, 2)
    lower = lax.rem(chip % 2 + (step + 1) // 2, 2)
    return upper * 2 + lower


def kernel(
    scaling,
    count,
    tok_ref,
    w_ref,
    high_ref,
    low_ref,
    twist_ref,
    last_ref,
    perm_ref,
    out_ref,
    tok_s,
    send_a,
    recv_a,
    zhigh,
    zlow,
    turned,
    send_b,
    recv_b,
    send_a_sem,
    recv_a_sem,
    send_b_sem,
    recv_b_sem,
):
    me = lax.axis_index("row")
    chip = me // 2
    chips = count // 2
    size = tok_ref.shape[0]
    groups = tok_ref.shape[1] // size
    inner = size // RADIX
    mid = size // 2
    barrier = pltpu.get_barrier_semaphore()
    for ahead in range(1, count):
        pl.semaphore_signal(
            barrier,
            inc=1,
            device_id={"row": lax.rem(me + ahead, count)},
            device_id_type=pl.DeviceIdType.MESH,
        )

    lane = lax.broadcasted_iota(jnp.int32, (1, LANES), 1)
    first = lane < HALF
    sign = jnp.where(first, 1.0, -1.0)

    for g in range(groups):
        cols = slice(g * size, (g + 1) * size)
        tok_s[:, cols] = dot(perm_ref[...], tok_ref[:, cols]).astype(jnp.bfloat16)

    def copy_a(target):
        return pltpu.make_async_remote_copy(
            src_ref=send_a.at[target],
            dst_ref=recv_a.at[me],
            send_sem=send_a_sem.at[target],
            recv_sem=recv_a_sem.at[me],
            device_id={"row": target},
            device_id_type=pl.DeviceIdType.MESH,
        )

    def copy_b(target):
        return pltpu.make_async_remote_copy(
            src_ref=send_b.at[target],
            dst_ref=recv_b.at[me],
            send_sem=send_b_sem.at[target],
            recv_sem=recv_b_sem.at[me],
            device_id={"row": target},
            device_id_type=pl.DeviceIdType.MESH,
        )

    pl.semaphore_wait(barrier, count - 1)

    @pl.loop(0, chips)
    def _(step):
        goal = peer_at(step, chip)
        cols = pl.ds(pl.multiple_of(goal * LANES, LANES), LANES)
        side = jnp.concatenate(
            [w_ref[g * size : (g + 1) * size, cols] for g in range(groups)], axis=1
        )
        folded = dot(high_ref[...], side) + dot(low_ref[...], side)
        total = None
        for g in range(groups):
            cosw = folded[:size, g * LANES : (g + 1) * LANES]
            sinw = -folded[size:, g * LANES : (g + 1) * LANES]
            pair = jnp.concatenate(
                [
                    jnp.where(first, cosw, pltpu.roll(sinw, HALF, 1)),
                    jnp.where(first, pltpu.roll(cosw, HALF, 1), sinw),
                ],
                axis=1,
            )
            high, low = split(pair)
            part = tok_s[:, g * size : (g + 1) * size]
            term = dot(part, high) + dot(part, low)
            total = term if total is None else total + term
        for core in range(2):
            target = goal * 2 + core
            block = total[:, core * LANES : (core + 1) * LANES]
            peak = jnp.max(jnp.abs(block), axis=1, keepdims=True)
            peak = jnp.max(peak, axis=0, keepdims=True)
            scale = jnp.broadcast_to(jnp.maximum(peak, 1e-30) * 1.0079, (EXTRA, LANES))
            scale = scale.astype(jnp.bfloat16)
            factor = CODE / scale[0:1].astype(jnp.float32)
            code = jnp.exp(jnp.abs(block) * factor) - 1.0
            code = jnp.where(block < 0.0, -code, code).astype(jnp.bfloat16)

            @pl.when(target != me)
            def _():
                send_a[target, :size] = code
                send_a[target, size:] = scale
                copy_a(target).start()

            @pl.when(target == me)
            def _():
                recv_a[target, :size] = code
                recv_a[target, size:] = scale

    @pl.loop(0, count)
    def _(at):
        source = peer_at(chips - 1 - at // 2, chip) * 2 + at % 2

        @pl.when(source != me)
        def _():
            pltpu.make_async_remote_copy(
                src_ref=send_a.at[source],
                dst_ref=recv_a.at[source],
                send_sem=send_a_sem.at[source],
                recv_sem=recv_a_sem.at[source],
                device_id={"row": source},
                device_id_type=pl.DeviceIdType.MESH,
            ).wait_recv()

        factor = recv_a[source, size:].astype(jnp.float32)[0:1] * (scaling / CODE)
        code = recv_a[source, :size].astype(jnp.float32)
        value = jnp.log(1.0 + jnp.abs(code)) * factor
        value = jnp.where(code < 0.0, -value, value)
        high, low = split(value)
        rows = pl.ds(pl.multiple_of(source * inner, inner), inner)
        for t in range(RADIX):
            zhigh[rows, t * LANES : (t + 1) * LANES] = high[t * inner : (t + 1) * inner]
            zlow[rows, t * LANES : (t + 1) * LANES] = low[t * inner : (t + 1) * inner]

    for pair in range(RADIX // 2):
        cols = slice(pair * 2 * LANES, (pair + 1) * 2 * LANES)
        found = dot(high_ref[...], zhigh[:, cols])
        found += dot(high_ref[...], zlow[:, cols])
        found += dot(low_ref[...], zhigh[:, cols])
        for half in range(2):
            t = pair * 2 + half
            cosz = found[:size, half * LANES : (half + 1) * LANES]
            sinz = found[size:, half * LANES : (half + 1) * LANES]
            whole = cosz + sign * pltpu.roll(sinz, HALF, 1)
            if t:
                whole = twist_ref[:, t : t + 1] * whole + (
                    twist_ref[:, RADIX + t : RADIX + t + 1] * sign
                ) * pltpu.roll(whole, HALF, 1)
            turned[t] = whole

    @pl.loop(0, count)
    def _(at):
        target = peer_at(at // 2, chip) * 2 + at % 2
        weights = last_ref[target]
        rows_at = 32
        for chunk in range(mid // rows_at):
            upper = slice(chunk * rows_at, (chunk + 1) * rows_at)
            under = slice(mid + chunk * rows_at, mid + (chunk + 1) * rows_at)
            top = weights[0:1] * turned[0, upper]
            bottom = weights[0:1] * turned[0, under]
            for t in range(1, RADIX):
                top += weights[t : t + 1] * turned[t, upper]
                bottom += weights[t : t + 1] * turned[t, under]
            packed = jnp.where(first, top, bottom) + pltpu.roll(
                jnp.where(first, bottom, top), HALF, 1
            )
            packed = packed.astype(jnp.bfloat16)
            send_b[target, upper] = packed

        @pl.when(target != me)
        def _():
            copy_b(target).start()

    recv_b[me] = send_b[me]

    for at in range(chips):
        goal = peer_at(chips - 1 - at, chip)
        for core in range(2):
            source = goal * 2 + core

            @pl.when(source != me)
            def _():
                pltpu.make_async_remote_copy(
                    src_ref=send_b.at[source],
                    dst_ref=recv_b.at[source],
                    send_sem=send_b_sem.at[source],
                    recv_sem=recv_b_sem.at[source],
                    device_id={"row": source},
                    device_id_type=pl.DeviceIdType.MESH,
                ).wait_recv()

        left = recv_b[goal * 2].astype(jnp.float32)
        right = recv_b[goal * 2 + 1].astype(jnp.float32)
        cols = pl.ds(pl.multiple_of(goal * LANES, LANES), LANES)
        out_ref[:mid, cols] = jnp.where(first, left, pltpu.roll(right, HALF, 1)).astype(
            jnp.bfloat16
        )
        out_ref[mid:, cols] = jnp.where(first, pltpu.roll(left, HALF, 1), right).astype(
            jnp.bfloat16
        )

    @pl.loop(1, count)
    def _(ahead):
        target = lax.rem(me + ahead, count)
        copy_a(target).wait_send()
        copy_b(target).wait_send()


def kernel_body(count, tokens, out_weight):
    size = tokens.shape[0]
    length = size * count
    scaling = 1.0 / math.sqrt(length * GROUP_DIM)
    vmem = pl.BlockSpec(memory_space=pltpu.VMEM)
    consts = [jnp.asarray(table) for table in tables(size, length)]
    return pl.pallas_call(
        functools.partial(kernel, scaling, count),
        out_shape=jax.ShapeDtypeStruct((size, out_weight.shape[1]), jnp.bfloat16),
        in_specs=[vmem] * (2 + len(consts)),
        out_specs=vmem,
        scratch_shapes=[
            pltpu.VMEM(tokens.shape, jnp.bfloat16),
            pltpu.VMEM((count, size + EXTRA, LANES), jnp.bfloat16),
            pltpu.VMEM((count, size + EXTRA, LANES), jnp.bfloat16),
            pltpu.VMEM((size, RADIX * LANES), jnp.bfloat16),
            pltpu.VMEM((size, RADIX * LANES), jnp.bfloat16),
            pltpu.VMEM((RADIX, size, LANES), jnp.float32),
            pltpu.VMEM((count, size // 2, LANES), jnp.bfloat16),
            pltpu.VMEM((count, size // 2, LANES), jnp.bfloat16),
            pltpu.SemaphoreType.DMA((count,)),
            pltpu.SemaphoreType.DMA((count,)),
            pltpu.SemaphoreType.DMA((count,)),
            pltpu.SemaphoreType.DMA((count,)),
        ],
        compiler_params=pltpu.CompilerParams(
            collective_id=0, has_side_effects=True, vmem_limit_bytes=60 * 1024 * 1024
        ),
    )(tokens, out_weight, *consts)


def body(tokens, out_weight):
    size = tokens.shape[0]
    count = lax.axis_size("row")
    fits = (
        count == RADIX
        and size == GROUP_DIM
        and tokens.shape[1] == GROUPS * GROUP_DIM
        and out_weight.shape[1] == count * HALF
    )
    if fits:
        return kernel_body(count, tokens, out_weight)
    return general_body(tokens, out_weight)


def solution(mesh):
    placed = (P("row", None), P(None, "col"))
    return jax.shard_map(
        body, mesh=mesh, in_specs=placed, out_specs=P("row", "col"), check_vma=False
    )
```

profile of v0, /device:TPU:9, one launch (start us, length us, event | category | flops | bytes accessed | tf_op | source)
XLA Modules:
  0.0 54.4 jit_solution(1675636115743874289)
XLA Ops:
  0.0 52.5 %shard_map.73 = bf16[512,512]{1,0:T(8,128)(2,1)} custom-call(bf16[512,2048]{1,0:T(8,128)(2,1)} %tok_ref.1, bf16[2048,512]{1,0:T(8,128)(2,1)} %w_ref.1, bf16[1024,512]{1,0:T(8,128)(2,1)} %constant.10.clone.high_ref, bf16[1024,512]{1,0:T(8,128)(2,1)} %constant.11.clone.low_ref, f32[512,128]{1,0:T(8,128)} %constant.12.clone.twist_ref, ...), custom_call_target="tpu_custom_call" | custom-call | tf_op jit(solution)/shard_map/pallas_call | solution.py:356
  52.5 1.9 %copy.9 = bf16[512,512]{1,0:T(8,128)(2,1)} copy(bf16[512,512]{1,0:T(8,128)(2,1)} %shard_map.73) | data formatting | bytes 1048576
where the time goes:
time: 54.6 us; the launch traced here: 54.4 us
  Pallas kernels  52.5 us (96%)
  local copies, waits for them, and re-layouts  1.87 us (3%)
    pallas_call x1, Pallas kernels, kernel_body(): pl.pallas_call(functools.partial(kernel, scaling, count), out_shape=jax.S...  52.5 us
    unnamed x1, local copies, waits for them, and re-layouts  1.87 us

commit v1 on v0

--- a/solution.py
+++ b/solution.py
@@ -86,6 +86,7 @@
 HALF = 64
 LANES = 128
 EXTRA = 16
+PARTS = 4
 CODE = 84.0
 
 
@@ -111,11 +112,7 @@
         ],
         axis=2,
     ).astype(np.float32)
-    inner = size // RADIX
-    perm = np.zeros((size, size), np.float32)
-    rows = np.arange(size)
-    perm[rows, (rows % inner) * RADIX + rows // inner] = 1.0
-    return high, low, twist, last, perm.astype(high.dtype)
+    return high, low, twist, last
 
 
 def dot(a, b):
@@ -128,22 +125,27 @@
 
 
 def peer_at(step, chip):
-    upper = lax.rem(chip // 2 + 1 - step // 2, 2)
-    lower = lax.rem(chip % 2 + (step + 1) // 2, 2)
-    return upper * 2 + lower
+    upper = chip // 2
+    folded = chip + upper * (3 - 2 * chip)
+    place = lax.rem(step + 1 + folded, 4)
+    goal = place + place // 2 - 2 * (place // 3)
+    return goal + upper * (3 - 2 * goal)
 
 
 def kernel(
     scaling,
     count,
+    tok_hbm,
+    w_hbm,
+    high_hbm,
+    low_hbm,
+    twist_ref,
+    last_ref,
+    out_ref,
     tok_ref,
     w_ref,
     high_ref,
     low_ref,
-    twist_ref,
-    last_ref,
-    perm_ref,
-    out_ref,
     tok_s,
     send_a,
     recv_a,
@@ -152,6 +154,7 @@
     turned,
     send_b,
     recv_b,
+    load_sem,
     send_a_sem,
     recv_a_sem,
     send_b_sem,
@@ -164,6 +167,13 @@
     groups = tok_ref.shape[1] // size
     inner = size // RADIX
     mid = size // 2
+    part_rows = size // PARTS
+    loads = []
+    for at, (source, target) in enumerate(
+        [(high_hbm, high_ref), (w_hbm, w_ref), (low_hbm, low_ref), (tok_hbm, tok_ref)]
+    ):
+        loads.append(pltpu.make_async_copy(source, target, load_sem.at[at]))
+        loads[-1].start()
     barrier = pltpu.get_barrier_semaphore()
     for ahead in range(1, count):
         pl.semaphore_signal(
@@ -177,16 +187,12 @@
     first = lane < HALF
     sign = jnp.where(first, 1.0, -1.0)
 
-    for g in range(groups):
-        cols = slice(g * size, (g + 1) * size)
-        tok_s[:, cols] = dot(perm_ref[...], tok_ref[:, cols]).astype(jnp.bfloat16)
-
-    def copy_a(target):
+    def copy_a(part, target):
         return pltpu.make_async_remote_copy(
-            src_ref=send_a.at[target],
-            dst_ref=recv_a.at[me],
-            send_sem=send_a_sem.at[target],
-            recv_sem=recv_a_sem.at[me],
+            src_ref=send_a.at[part, target],
+            dst_ref=recv_a.at[part, me],
+            send_sem=send_a_sem.at[part, target],
+            recv_sem=recv_a_sem.at[part, me],
             device_id={"row": target},
             device_id_type=pl.DeviceIdType.MESH,
         )
@@ -201,7 +207,8 @@
             device_id_type=pl.DeviceIdType.MESH,
         )
 
-    pl.semaphore_wait(barrier, count - 1)
+    for load in loads[:3]:
+        load.wait()
 
     @pl.loop(0, chips)
     def _(step):
@@ -211,6 +218,18 @@
             [w_ref[g * size : (g + 1) * size, cols] for g in range(groups)], axis=1
         )
         folded = dot(high_ref[...], side) + dot(low_ref[...], side)
+
+        @pl.when(step == 0)
+        def _():
+            loads[3].wait()
+            spot = lax.broadcasted_iota(jnp.int32, (size, size), 0)
+            spot = (spot % inner) * RADIX + spot // inner
+            place = lax.broadcasted_iota(jnp.int32, (size, size), 1)
+            perm = jnp.where(spot == place, 1.0, 0.0).astype(jnp.bfloat16)
+            for g in range(groups):
+                span = slice(g * size, (g + 1) * size)
+                tok_s[:, span] = dot(perm, tok_ref[:, span]).astype(jnp.bfloat16)
+
         total = None
         for g in range(groups):
             cosw = folded[:size, g * LANES : (g + 1) * LANES]
@@ -236,44 +255,69 @@
             factor = CODE / scale[0:1].astype(jnp.float32)
             code = jnp.exp(jnp.abs(block) * factor) - 1.0
             code = jnp.where(block < 0.0, -code, code).astype(jnp.bfloat16)
-
-            @pl.when(target != me)
+            for part in range(PARTS):
+                rows = slice(part * part_rows, (part + 1) * part_rows)
+                send_a[part, target, :part_rows] = code[rows]
+                send_a[part, target, part_rows:] = scale
+
+        def ship(parts, steps):
+            for part in parts:
+                for at in steps:
+                    for core in range(2):
+                        copy_a(part, peer_at(at, chip) * 2 + core).start()
+
+        half = range(PARTS // 2)
+        rest = range(PARTS // 2, PARTS)
+
+        @pl.when(step == 0)
+        def _():
+            pl.semaphore_wait(barrier, count - 1)
+            ship(half, [0])
+
+        @pl.when(step == 1)
+        def _():
+            ship(half, [1])
+
+        @pl.when(step == 2)
+        def _():
+            ship(half, [2])
+            ship(rest, [0, 1, 2])
+
+        @pl.when(step == chips - 1)
+        def _():
+            for part in range(PARTS):
+                copy_a(part, chip * 2 + (1 - me % 2)).start()
+                recv_a[part, me] = send_a[part, me]
+
+    for pair in range(RADIX // 2):
+
+        @pl.loop(0, count)
+        def _(at):
+            source = peer_at(chips - 1 - at // 2, chip) * 2 + at % 2
+
+            @pl.when(source != me)
             def _():
-                send_a[target, :size] = code
-                send_a[target, size:] = scale
-                copy_a(target).start()
-
-            @pl.when(target == me)
-            def _():
-                recv_a[target, :size] = code
-                recv_a[target, size:] = scale
-
-    @pl.loop(0, count)
-    def _(at):
-        source = peer_at(chips - 1 - at // 2, chip) * 2 + at % 2
-
-        @pl.when(source != me)
-        def _():
-            pltpu.make_async_remote_copy(
-                src_ref=send_a.at[source],
-                dst_ref=recv_a.at[source],
-                send_sem=send_a_sem.at[source],
-                recv_sem=recv_a_sem.at[source],
-                device_id={"row": source},
-                device_id_type=pl.DeviceIdType.MESH,
-            ).wait_recv()
-
-        factor = recv_a[source, size:].astype(jnp.float32)[0:1] * (scaling / CODE)
-        code = recv_a[source, :size].astype(jnp.float32)
-        value = jnp.log(1.0 + jnp.abs(code)) * factor
-        value = jnp.where(code < 0.0, -value, value)
-        high, low = split(value)
-        rows = pl.ds(pl.multiple_of(source * inner, inner), inner)
-        for t in range(RADIX):
-            zhigh[rows, t * LANES : (t + 1) * LANES] = high[t * inner : (t + 1) * inner]
-            zlow[rows, t * LANES : (t + 1) * LANES] = low[t * inner : (t + 1) * inner]
-
-    for pair in range(RADIX // 2):
+                pltpu.make_async_remote_copy(
+                    src_ref=send_a.at[pair, source],
+                    dst_ref=recv_a.at[pair, source],
+                    send_sem=send_a_sem.at[pair, source],
+                    recv_sem=recv_a_sem.at[pair, source],
+                    device_id={"row": source},
+                    device_id_type=pl.DeviceIdType.MESH,
+                ).wait_recv()
+
+            factor = recv_a[pair, source, part_rows:].astype(jnp.float32)[0:1]
+            factor = factor * (scaling / CODE)
+            code = recv_a[pair, source, :part_rows].astype(jnp.float32)
+            value = jnp.log(1.0 + jnp.abs(code)) * factor
+            value = jnp.where(code < 0.0, -value, value)
+            high, low = split(value)
+            rows = pl.ds(pl.multiple_of(source * inner, inner), inner)
+            for half in range(2):
+                span = slice((pair * 2 + half) * LANES, (pair * 2 + half + 1) * LANES)
+                zhigh[rows, span] = high[half * inner : (half + 1) * inner]
+                zlow[rows, span] = low[half * inner : (half + 1) * inner]
+
         cols = slice(pair * 2 * LANES, (pair + 1) * 2 * LANES)
         found = dot(high_ref[...], zhigh[:, cols])
         found += dot(high_ref[...], zlow[:, cols])
@@ -343,7 +387,8 @@
     @pl.loop(1, count)
     def _(ahead):
         target = lax.rem(me + ahead, count)
-        copy_a(target).wait_send()
+        for part in range(PARTS):
+            copy_a(part, target).wait_send()
         copy_b(target).wait_send()
 
 
@@ -356,19 +401,24 @@
     return pl.pallas_call(
         functools.partial(kernel, scaling, count),
         out_shape=jax.ShapeDtypeStruct((size, out_weight.shape[1]), jnp.bfloat16),
-        in_specs=[vmem] * (2 + len(consts)),
+        in_specs=[pl.BlockSpec(memory_space=pl.ANY)] * 4 + [vmem] * 2,
         out_specs=vmem,
         scratch_shapes=[
             pltpu.VMEM(tokens.shape, jnp.bfloat16),
-            pltpu.VMEM((count, size + EXTRA, LANES), jnp.bfloat16),
-            pltpu.VMEM((count, size + EXTRA, LANES), jnp.bfloat16),
+            pltpu.VMEM(out_weight.shape, jnp.bfloat16),
+            pltpu.VMEM((2 * size, size), jnp.bfloat16),
+            pltpu.VMEM((2 * size, size), jnp.bfloat16),
+            pltpu.VMEM(tokens.shape, jnp.bfloat16),
+            pltpu.VMEM((PARTS, count, size // PARTS + EXTRA, LANES), jnp.bfloat16),
+            pltpu.VMEM((PARTS, count, size // PARTS + EXTRA, LANES), jnp.bfloat16),
             pltpu.VMEM((size, RADIX * LANES), jnp.bfloat16),
             pltpu.VMEM((size, RADIX * LANES), jnp.bfloat16),
             pltpu.VMEM((RADIX, size, LANES), jnp.float32),
             pltpu.VMEM((count, size // 2, LANES), jnp.bfloat16),
             pltpu.VMEM((count, size // 2, LANES), jnp.bfloat16),
-            pltpu.SemaphoreType.DMA((count,)),
-            pltpu.SemaphoreType.DMA((count,)),
+            pltpu.SemaphoreType.DMA((4,)),
+            pltpu.SemaphoreType.DMA((PARTS, count)),
+            pltpu.SemaphoreType.DMA((PARTS, count)),
             pltpu.SemaphoreType.DMA((count,)),
             pltpu.SemaphoreType.DMA((count,)),
         ],

time: 54.6 us -> 54.2 us (level)
  no operation moved by 1% of the time
where the time goes in v1:
time: 54.2 us; the launch traced here: 54 us
  Pallas kernels  52.1 us (96%)
  local copies, waits for them, and re-layouts  1.87 us (3%)
    pallas_call x1, Pallas kernels, kernel_body(): pl.pallas_call(functools.partial(kernel, scaling, count), out_shape=jax.S...  52.1 us
    unnamed x1, local copies, waits for them, and re-layouts  1.87 us

profile of v1, /device:TPU:9, one launch (start us, length us, event | category | flops | bytes accessed | tf_op | source)
XLA Modules:
  0.0 54.0 jit_solution(10431497387312583454)
XLA Ops:
  0.0 52.1 %shard_map.64 = bf16[512,512]{1,0:T(8,128)(2,1)} custom-call(bf16[512,2048]{1,0:T(8,128)(2,1)} %tok_hbm.1, bf16[2048,512]{1,0:T(8,128)(2,1)} %w_hbm.1, bf16[1024,512]{1,0:T(8,128)(2,1)} %constant.8.clone.high_hbm, bf16[1024,512]{1,0:T(8,128)(2,1)} %constant.9.clone.low_hbm, f32[512,128]{1,0:T(8,128)} %constant.10.clone.twist_ref, ...), custom_call_target="tpu_custom_call" | custom-call | tf_op jit(solution)/shard_map/pallas_call | solution.py:401
  52.1 1.9 %copy.8 = bf16[512,512]{1,0:T(8,128)(2,1)} copy(bf16[512,512]{1,0:T(8,128)(2,1)} %shard_map.64) | data formatting | bytes 1048576

commit v2 on v1

--- a/solution.py
+++ b/solution.py
@@ -152,6 +152,7 @@
     zhigh,
     zlow,
     turned,
+    found_s,
     send_b,
     recv_b,
     load_sem,
@@ -170,10 +171,22 @@
     part_rows = size // PARTS
     loads = []
     for at, (source, target) in enumerate(
-        [(high_hbm, high_ref), (w_hbm, w_ref), (low_hbm, low_ref), (tok_hbm, tok_ref)]
+        [(high_hbm, high_ref), (low_hbm, low_ref), (tok_hbm, tok_ref)]
     ):
         loads.append(pltpu.make_async_copy(source, target, load_sem.at[at]))
-        loads[-1].start()
+
+    def load_w(step):
+        goal = peer_at(step, chip)
+        cols = pl.ds(pl.multiple_of(goal * LANES, LANES), LANES)
+        return pltpu.make_async_copy(
+            w_hbm.at[:, cols], w_ref.at[:, cols], load_sem.at[3 + step]
+        )
+
+    load_w(0).start()
+    for load in loads:
+        load.start()
+    for step in range(1, 4):
+        load_w(step).start()
     barrier = pltpu.get_barrier_semaphore()
     for ahead in range(1, count):
         pl.semaphore_signal(
@@ -207,13 +220,14 @@
             device_id_type=pl.DeviceIdType.MESH,
         )
 
-    for load in loads[:3]:
+    for load in loads[:2]:
         load.wait()
 
     @pl.loop(0, chips)
     def _(step):
         goal = peer_at(step, chip)
         cols = pl.ds(pl.multiple_of(goal * LANES, LANES), LANES)
+        load_w(step).wait()
         side = jnp.concatenate(
             [w_ref[g * size : (g + 1) * size, cols] for g in range(groups)], axis=1
         )
@@ -221,10 +235,10 @@
 
         @pl.when(step == 0)
         def _():
-            loads[3].wait()
+            loads[2].wait()
+            place = lax.broadcasted_iota(jnp.int32, (1, size), 1)
+            place = (place % RADIX) * inner + place // RADIX
             spot = lax.broadcasted_iota(jnp.int32, (size, size), 0)
-            spot = (spot % inner) * RADIX + spot // inner
-            place = lax.broadcasted_iota(jnp.int32, (size, size), 1)
             perm = jnp.where(spot == place, 1.0, 0.0).astype(jnp.bfloat16)
             for g in range(groups):
                 span = slice(g * size, (g + 1) * size)
@@ -291,9 +305,8 @@
 
     for pair in range(RADIX // 2):
 
-        @pl.loop(0, count)
-        def _(at):
-            source = peer_at(chips - 1 - at // 2, chip) * 2 + at % 2
+        def take(at, base):
+            source = base + at
 
             @pl.when(source != me)
             def _():
@@ -318,10 +331,17 @@
                 zhigh[rows, span] = high[half * inner : (half + 1) * inner]
                 zlow[rows, span] = low[half * inner : (half + 1) * inner]
 
+        def near_or_far(base):
+            pl.loop(0, count // 2)(lambda at: take(at, base))
+            span = pl.ds(pl.multiple_of(base * inner, size // 2), size // 2)
+            terms = dot(high_ref[:, span], zhigh[span, cols])
+            terms += dot(high_ref[:, span], zlow[span, cols])
+            return terms + dot(low_ref[:, span], zhigh[span, cols])
+
         cols = slice(pair * 2 * LANES, (pair + 1) * 2 * LANES)
-        found = dot(high_ref[...], zhigh[:, cols])
-        found += dot(high_ref[...], zlow[:, cols])
-        found += dot(low_ref[...], zhigh[:, cols])
+        own = (me // (count // 2)) * (count // 2)
+        found_s[...] = near_or_far(own)
+        found = found_s[...] + near_or_far(count // 2 - own)
         for half in range(2):
             t = pair * 2 + half
             cosz = found[:size, half * LANES : (half + 1) * LANES]
@@ -414,9 +434,10 @@
             pltpu.VMEM((size, RADIX * LANES), jnp.bfloat16),
             pltpu.VMEM((size, RADIX * LANES), jnp.bfloat16),
             pltpu.VMEM((RADIX, size, LANES), jnp.float32),
+            pltpu.VMEM((2 * size, 2 * LANES), jnp.float32),
             pltpu.VMEM((count, size // 2, LANES), jnp.bfloat16),
             pltpu.VMEM((count, size // 2, LANES), jnp.bfloat16),
-            pltpu.SemaphoreType.DMA((4,)),
+            pltpu.SemaphoreType.DMA((7,)),
             pltpu.SemaphoreType.DMA((PARTS, count)),
             pltpu.SemaphoreType.DMA((PARTS, count)),
             pltpu.SemaphoreType.DMA((count,)),

time: 54.2 us -> 52.8 us (0.974)
  Pallas kernels: 52.1 us -> 50.6 us
    pallas_call x1, Pallas kernels: 52.1 us -> 50.6 us  [kernel_body(): pl.pallas_call(functools.partial(kernel, scaling, count), out_shape=jax.S...]
where the time goes in v2:
time: 52.8 us; the launch traced here: 52.5 us
  Pallas kernels  50.6 us (96%)
  local copies, waits for them, and re-layouts  1.87 us (4%)
    pallas_call x1, Pallas kernels, kernel_body(): pl.pallas_call(functools.partial(kernel, scaling, count), out_shape=jax.S...  50.6 us
    unnamed x1, local copies, waits for them, and re-layouts  1.87 us

profile of v2, /device:TPU:9, one launch (start us, length us, event | category | flops | bytes accessed | tf_op | source)
XLA Modules:
  0.0 52.5 jit_solution(105778329592757809)
XLA Ops:
  0.0 50.6 %shard_map.64 = bf16[512,512]{1,0:T(8,128)(2,1)} custom-call(bf16[512,2048]{1,0:T(8,128)(2,1)} %tok_hbm.1, bf16[2048,512]{1,0:T(8,128)(2,1)} %w_hbm.1, bf16[1024,512]{1,0:T(8,128)(2,1)} %constant.8.clone.high_hbm, bf16[1024,512]{1,0:T(8,128)(2,1)} %constant.9.clone.low_hbm, f32[512,128]{1,0:T(8,128)} %constant.10.clone.twist_ref, ...), custom_call_target="tpu_custom_call" | custom-call | tf_op jit(solution)/shard_map/pallas_call | solution.py:421
  50.6 1.9 %copy.8 = bf16[512,512]{1,0:T(8,128)(2,1)} copy(bf16[512,512]{1,0:T(8,128)(2,1)} %shard_map.64) | data formatting | bytes 1048576

commit v3 on v2

--- a/solution.py
+++ b/solution.py
@@ -153,6 +153,8 @@
     zlow,
     turned,
     found_s,
+    fold_high,
+    fold_low,
     send_b,
     recv_b,
     load_sem,
@@ -244,7 +246,6 @@
                 span = slice(g * size, (g + 1) * size)
                 tok_s[:, span] = dot(perm, tok_ref[:, span]).astype(jnp.bfloat16)
 
-        total = None
         for g in range(groups):
             cosw = folded[:size, g * LANES : (g + 1) * LANES]
             sinw = -folded[size:, g * LANES : (g + 1) * LANES]
@@ -256,9 +257,9 @@
                 axis=1,
             )
             high, low = split(pair)
-            part = tok_s[:, g * size : (g + 1) * size]
-            term = dot(part, high) + dot(part, low)
-            total = term if total is None else total + term
+            fold_high[g * size : (g + 1) * size] = high
+            fold_low[g * size : (g + 1) * size] = low
+        total = dot(tok_s[...], fold_high[...]) + dot(tok_s[...], fold_low[...])
         for core in range(2):
             target = goal * 2 + core
             block = total[:, core * LANES : (core + 1) * LANES]
@@ -291,11 +292,13 @@
         @pl.when(step == 1)
         def _():
             ship(half, [1])
+            ship(range(PARTS // 2, PARTS - 1), [0, 1])
 
         @pl.when(step == 2)
         def _():
             ship(half, [2])
-            ship(rest, [0, 1, 2])
+            ship(range(PARTS // 2, PARTS - 1), [2])
+            ship(range(PARTS - 1, PARTS), [0, 1, 2])
 
         @pl.when(step == chips - 1)
         def _():
@@ -435,6 +438,8 @@
             pltpu.VMEM((size, RADIX * LANES), jnp.bfloat16),
             pltpu.VMEM((RADIX, size, LANES), jnp.float32),
             pltpu.VMEM((2 * size, 2 * LANES), jnp.float32),
+            pltpu.VMEM((tokens.shape[1], 2 * LANES), jnp.bfloat16),
+            pltpu.VMEM((tokens.shape[1], 2 * LANES), jnp.bfloat16),
             pltpu.VMEM((count, size // 2, LANES), jnp.bfloat16),
             pltpu.VMEM((count, size // 2, LANES), jnp.bfloat16),
             pltpu.SemaphoreType.DMA((7,)),

time: 52.8 us -> 52.5 us (level)
  no operation moved by 1% of the time
where the time goes in v3:
time: 52.5 us; the launch traced here: 52.4 us
  Pallas kernels  50.5 us (96%)
  local copies, waits for them, and re-layouts  1.87 us (4%)
    pallas_call x1, Pallas kernels, kernel_body(): pl.pallas_call(functools.partial(kernel, scaling, count), out_shape=jax.S...  50.5 us
    unnamed x1, local copies, waits for them, and re-layouts  1.87 us

profile of v3, /device:TPU:9, one launch (start us, length us, event | category | flops | bytes accessed | tf_op | source)
XLA Modules:
  0.0 52.4 jit_solution(3222545057575129155)
XLA Ops:
  0.0 50.5 %shard_map.64 = bf16[512,512]{1,0:T(8,128)(2,1)} custom-call(bf16[512,2048]{1,0:T(8,128)(2,1)} %tok_hbm.1, bf16[2048,512]{1,0:T(8,128)(2,1)} %w_hbm.1, bf16[1024,512]{1,0:T(8,128)(2,1)} %constant.8.clone.high_hbm, bf16[1024,512]{1,0:T(8,128)(2,1)} %constant.9.clone.low_hbm, f32[512,128]{1,0:T(8,128)} %constant.10.clone.twist_ref, ...), custom_call_target="tpu_custom_call" | custom-call | tf_op jit(solution)/shard_map/pallas_call | solution.py:424
  50.5 1.9 %copy.8 = bf16[512,512]{1,0:T(8,128)(2,1)} copy(bf16[512,512]{1,0:T(8,128)(2,1)} %shard_map.64) | data formatting | bytes 1048576
